TPU v7x, 32 devices: a whole 2x2x4 slice. The times are simulated.
32 devices in a mesh: grp: 2 (over y), sp: 4 (over z), tp: 4 (over x, core).
Axes of the slice: x: 2, y: 2, z: 4, core: 2. Of those that a mesh axis runs over, the one named last changes fastest.
Arguments:
- residual: bfloat16 [2048, 2048], P(('grp', 'sp')), parts along dimension 0, may hold values from -34 to 34
- queries: bfloat16 [2048, 1024], P(('grp', 'sp'), 'tp'), parts along dimension 0, may hold values from -400 to 400
- keys: bfloat16 [2048, 512], P(('grp', 'sp'), 'tp'), parts along dimension 0, may hold values from -8 to 8
- values: bfloat16 [2048, 512], P(('grp', 'sp'), 'tp'), parts along dimension 0, may hold values from -6 to 6
- segments: int32 [2048], P(('grp', 'sp')), parts along dimension 0, may hold values from 0 to 2, never falling along the last dimension, each value on 1 to 768 neighbouring positions
- routes: int32 [2048, 2], P(('grp', 'sp')), parts along dimension 0, may hold values from 0 to 3, all different within a row; in each aligned block of 256 rows (0 to 255, 256 to 511, ...) at most 256 rows name the same one
- route_weight: float32 [2048, 2], P(('grp', 'sp')), parts along dimension 0, may hold values from 0.3 to 3
- sinks: float32 [16], P('tp'), may hold values from 1 to 6
- out_weight: bfloat16 [1024, 2048], P('tp'), may hold values from -1 to 1
- norm_gain: float32 [2048], replicated, may hold values from 0.1 to 1.9
- expert_gate: bfloat16 [4, 2048, 1024], P('sp', None, 'tp'), may hold values from -0.125 to 0.125
- expert_up: bfloat16 [4, 2048, 1024], P('sp', None, 'tp'), may hold values from -0.125 to 0.125
- expert_down: bfloat16 [4, 1024, 2048], P('sp', None, 'tp'), may hold values from -0.1875 to 0.1875
- shared_gate: bfloat16 [2048, 1024], P(None, 'tp'), may hold values from -0.125 to 0.125
- shared_up: bfloat16 [2048, 1024], P(None, 'tp'), may hold values from -0.125 to 0.125
- shared_down: bfloat16 [1024, 2048], P(None, 'tp'), may hold values from -0.1875 to 0.1875
Outputs:
- mixed: bfloat16 [2048, 2048], P(('grp', 'sp'), 'tp'), parts along dimension 0
There are 2 independent parts, one for each index of `grp`. A program takes and returns all parts, laid end to end along the dimension named above; an argument that names none is the same for every part. Nothing has to cross between parts.
Inputs may be any that keep to these rules, and one draw needn't show every extreme that they name: `routes`: each row names 2 different experts. In the rows of one device no expert is named by more than 256 rows, and in some device's rows an expert is named by exactly 256. `segments`: document numbers never fall along the positions; every document spans 1 to 768 positions and one spans exactly 768.
All inputs are finite; a program needn't handle non-finite values.
Results may differ from a plain program's by a relative error of at most 0.0065.
Values may be sent and summed in bfloat16 or wider, within the bound.
A program may use at most 64 MiB of HBM per device.

v0:
```python
import jax
import jax.numpy as jnp
from jax import lax
from jax.sharding import PartitionSpec as P

HEAD_DIM = 64
WINDOW = 128


epsilon = 1e-06


def passed_along(value, axis, steps):
    count = lax.axis_size(axis)
    leading, last = (max(0, -steps), min(count, count - steps))
    return lax.ppermute(value, axis, [(source, source + steps) for source in range(leading, last)])


def banded(prev_rows, own_rows, window_len):
    blocks = own_rows.shape[0] // window_len
    joined = jnp.concatenate([prev_rows, own_rows], axis=0)
    shaped = joined.reshape((blocks + 1, window_len) + own_rows.shape[1:])
    return jnp.concatenate([shaped[:-1], shaped[1:]], axis=1)


def shards(
    residual,
    queries,
    keys,
    values,
    segments,
    routes,
    route_weight,
    sinks,
    out_weight,
    norm_gain,
    expert_gate,
    expert_up,
    expert_down,
    shared_gate,
    shared_up,
    shared_down,
):
    rows_here = residual.shape[0]
    model_width = residual.shape[1]
    tp_count = lax.axis_size("tp")
    tp_index = lax.axis_index("tp")
    head_local = queries.shape[1] // HEAD_DIM
    kv_local = keys.shape[1] // HEAD_DIM
    group_size = head_local // kv_local
    window_len = WINDOW
    blocks = rows_here // window_len
    own_marks = (segments % 256 + 1).astype(jnp.bfloat16)
    prev_keys, prev_values, prev_marks = passed_along(
        (
            keys[rows_here - window_len :],
            values[rows_here - window_len :],
            own_marks[rows_here - window_len :],
        ),
        "sp",
        1,
    )
    key_band = banded(prev_keys, keys, window_len).reshape(
        blocks, 2 * window_len, kv_local, HEAD_DIM
    )
    value_band = banded(prev_values, values, window_len).reshape(
        blocks, 2 * window_len, kv_local, HEAD_DIM
    )
    mark_band = banded(prev_marks, own_marks, window_len).astype(jnp.float32)
    query_marks = own_marks.reshape(blocks, window_len).astype(jnp.float32)
    query_blocks = queries.reshape(blocks, window_len, kv_local, group_size, HEAD_DIM)
    scores = jnp.einsum(
        "nqhgd,nkhd->nhgqk", query_blocks, key_band, preferred_element_type=jnp.float32
    ) * HEAD_DIM ** (-0.5)
    offsets = jnp.arange(window_len)[:, None] + window_len - jnp.arange(2 * window_len)[None, :]
    allowed = (
        (offsets >= 0) & (offsets < window_len) & (query_marks[:, :, None] == mark_band[:, None, :])
    )
    sink_logits = sinks.reshape(kv_local, group_size)[None, :, :, None]
    masked = jnp.where(allowed[:, None, None], scores, -jnp.inf)
    top_score = jnp.maximum(jnp.max(masked, axis=-1), sink_logits)
    exp_terms = jnp.where(allowed[:, None, None], jnp.exp(scores - top_score[..., None]), 0.0)
    denominator = jnp.sum(exp_terms, axis=-1) + jnp.exp(sink_logits - top_score)
    probabilities = (exp_terms / denominator[..., None]).astype(jnp.bfloat16)
    attended = jnp.einsum(
        "nhgqk,nkhd->nqhgd", probabilities, value_band, preferred_element_type=jnp.float32
    )
    attended = attended.astype(jnp.bfloat16).reshape(rows_here, head_local * HEAD_DIM)
    partial_value = jnp.dot(attended, out_weight, preferred_element_type=jnp.float32)
    col_width = model_width // tp_count
    col_start = tp_index * col_width
    summed = lax.psum(partial_value, "tp")
    updated = (residual.astype(jnp.float32) + summed).astype(jnp.bfloat16)
    updated_f32 = updated.astype(jnp.float32)
    inv_rms = lax.rsqrt(jnp.mean(updated_f32 * updated_f32, axis=-1, keepdims=True) + epsilon)
    normed = (updated_f32 * inv_rms * norm_gain).astype(jnp.bfloat16)
    updated_cols = lax.dynamic_slice_in_dim(updated, col_start, col_width, 1)
    normed_cols = lax.dynamic_slice_in_dim(normed, col_start, col_width, 1)
    shared_pre = jnp.dot(normed, shared_gate, preferred_element_type=jnp.float32)
    shared_lin = jnp.dot(normed, shared_up, preferred_element_type=jnp.float32)
    shared_act = (jax.nn.silu(shared_pre) * shared_lin).astype(jnp.bfloat16)
    top_count = routes.shape[1]
    experts = lax.axis_size("sp")
    capacity = 2 * rows_here * top_count // experts
    flat_ids = routes.reshape(-1)
    one_hot = (flat_ids[:, None] == jnp.arange(experts, dtype=jnp.int32)[None, :]).astype(jnp.int32)
    rank_in = jnp.cumsum(one_hot, axis=0) - one_hot
    slot_dest = flat_ids * capacity + jnp.sum(rank_in * one_hot, axis=1)
    token_of = jnp.arange(rows_here * top_count, dtype=jnp.int32) // top_count
    slot_token = jnp.full((experts * capacity,), -1, jnp.int32).at[slot_dest].set(token_of)
    filled = slot_token >= 0
    safe_token = jnp.where(filled, slot_token, 0)
    outgoing = jnp.where(filled[:, None], normed_cols[safe_token], jnp.zeros((), jnp.bfloat16))
    pieces = lax.all_to_all(
        outgoing.reshape(experts, capacity, col_width),
        "sp",
        split_axis=0,
        concat_axis=0,
        tiled=True,
    )
    arrived = lax.all_gather(pieces, "tp", axis=2, tiled=True)
    expert_rows = arrived.reshape(-1, model_width)
    gate_pre = jnp.dot(expert_rows, expert_gate[0], preferred_element_type=jnp.float32)
    up_lin = jnp.dot(expert_rows, expert_up[0], preferred_element_type=jnp.float32)
    expert_act = (jax.nn.silu(gate_pre) * up_lin).astype(jnp.bfloat16)
    gathered_expert, gathered_shared = (
        lax.all_gather(expert_act, "tp", axis=1, tiled=True),
        lax.all_gather(shared_act, "tp", axis=1, tiled=True),
    )
    expert_out = jnp.dot(
        gathered_expert, expert_down[0], preferred_element_type=jnp.float32
    ).astype(jnp.bfloat16)
    returned = lax.all_to_all(
        expert_out.reshape(experts, capacity, col_width),
        "sp",
        split_axis=0,
        concat_axis=0,
        tiled=True,
    )
    returned = returned.reshape(experts * capacity, col_width)
    picked = returned[slot_dest].astype(jnp.float32).reshape(rows_here, top_count, col_width)
    routed = jnp.sum(picked * route_weight[:, :, None], axis=1)
    shared_cols = jnp.dot(gathered_shared, shared_down, preferred_element_type=jnp.float32)
    return (updated_cols.astype(jnp.float32) + shared_cols + routed).astype(jnp.bfloat16)


def solution(mesh):
    placed = (
        P(("grp", "sp"), None),
        P(("grp", "sp"), "tp"),
        P(("grp", "sp"), "tp"),
        P(("grp", "sp"), "tp"),
        P(("grp", "sp")),
        P(("grp", "sp"), None),
        P(("grp", "sp"), None),
        P("tp"),
        P("tp", None),
        P(),
        P("sp", None, "tp"),
        P("sp", None, "tp"),
        P("sp", None, "tp"),
        P(None, "tp"),
        P(None, "tp"),
        P(None, "tp"),
    )
    return jax.shard_map(
        shards, mesh=mesh, in_specs=placed, out_specs=P(("grp", "sp"), "tp"), check_vma=False
    )
```

profile of v0, /device:TPU:0, one launch (start us, length us, event | category | flops | bytes accessed | tf_op | source)
XLA Modules:
  0.0 231.0 jit_solution(2736606239957524361)
XLA Ops:
  6.5 0.8 bitcast_convert_fusion
  7.3 5.0 %collective-permute-start.1 = (bf16[128]{0:T(256)(128)(2,1)S(1)}, bf16[128]{0:T(256)(128)(2,1)S(1)}, u32[]{:S(2)}, u32[]{:S(2)}) collective-permute-start(bf16[128]{0:T(256)(128)(2,1)S(1)} %slice.47), channel_id=1, source_target_pairs={{0,4},{4,8},{8,12},{1,5},{5,9},{9,13},{2,6},{6,10},{10,14},{3,7},{... | collective-permute-start | bytes 776 | tf_op jit(solution)/shard_map/ppermute | solution.py:16
  12.3 0.8 slice.50
  13.1 3.5 %collective-permute-start.2 = (bf16[128,128]{1,0:T(8,128)(2,1)S(1)}, bf16[128,128]{1,0:T(8,128)(2,1)S(1)}, u32[]{:S(2)}, u32[]{:S(2)}) collective-permute-start(bf16[128,128]{1,0:T(8,128)(2,1)S(1)} %slice.50), channel_id=1, source_target_pairs={{0,4},{4,8},{8,12},{1,5},{5,9},{9,13},{2,6},{6,10},{10,14},{3,7},{... | collective-permute-start | bytes 98312 | tf_op jit(solution)/shard_map/ppermute | solution.py:16
  16.5 0.8 slice.45
  17.3 3.5 %collective-permute-start = (bf16[128,128]{1,0:T(8,128)(2,1)S(1)}, bf16[128,128]{1,0:T(8,128)(2,1)S(1)}, u32[]{:S(2)}, u32[]{:S(2)}) collective-permute-start(bf16[128,128]{1,0:T(8,128)(2,1)S(1)} %slice.45), channel_id=1, source_target_pairs={{0,4},{4,8},{8,12},{1,5},{5,9},{9,13},{2,6},{6,10},{10,14},{3,7},{... | collective-permute-start | bytes 98312 | tf_op jit(solution)/shard_map/ppermute | solution.py:16
  20.8 0.9 reshape.215
  21.7 0.9 reshape.213
  22.7 0.8 copy.33
  23.5 0.7 broadcast_multiply_fusion
  24.2 0.1 eq.51
  24.4 1.2 reduce-window.6
  25.6 0.2 slice_reduce_fusion
  25.8 1.1 reshape.216
  27.1 0.7 max.17
  28.0 0.1 compare_and_fusion
  28.1 0.8 pad_maximum_fusion
  29.1 0.4 select_reduce_fusion
  29.5 0.2 fusion.13
  30.1 0.4 fusion.8
  30.4 0.1 copy.31
  30.6 1.8 fusion.15
  32.5 0.1 eq.47
  32.6 0.2 reduce-window.9
  32.9 0.1 mul.85
  33.2 2.4 %scatter_custom_fusion = s32[1024]{0:T(1024)S(1)} fusion(s32[512]{0:T(512)S(1)} %bitcast.75, s32[512]{0:T(512)S(1)} %add_select_fusion, s32[]{:T(128)} %constant.70.clone.1), kind=kCustom, calls=%fused_computation.71 | custom fusion | bytes 4100 | tf_op jit(solution)/shard_map/scatter | solution.py:110
  35.7 46.5 %all-reduce.2.cloned.1.call-done = f32[256,2048]{1,0:T(8,128)} async-done(((f32[256,2048]{1,0:T(8,128)}), f32[256,2048]{1,0:T(8,128)}) %all-reduce.2.cloned.1.call-update) | async-done | bytes 2097168 | tf_op jit(solution)/shard_map/psum | solution.py:92
  82.2 2.0 fusion
  84.2 0.3 fusion.2
  84.5 1.0 copy-done.1
  85.5 4.0 %gather_fusion = bf16[1024,512]{1,0:T(8,128)(2,1)S(1)} fusion(bf16[256,512]{1,0:T(8,128)(2,1)S(1)} %constant_dynamic-slice_fusion, s32[1024]{0:T(1024)S(1)} %fusion.29), kind=kCustom, calls=%fused_computation | custom fusion | bytes 2101248 | tf_op jit(solution)/shard_map/gather | solution.py:113
  89.4 0.2 broadcast_select_fusion
  89.7 30.1 %all_to_all.10 = bf16[4,256,512]{2,1,0:T(8,128)(2,1)} all-to-all(bf16[4,256,512]{2,1,0:T(8,128)(2,1)S(1)} %broadcast_select_fusion), channel_id=1, replica_groups=mesh['grp'=2,'sp'=4,'tp'=4] {'sp'}, dimensions={0} | all-to-all | bytes 2097152 | tf_op jit(solution)/shard_map/all_to_all | solution.py:114
  119.9 32.9 %all-gather.3.cloned.1.call-done = bf16[4,256,2048]{2,1,0:T(8,128)(2,1)} async-done(((bf16[4,256,512]{2,1,0:T(8,128)(2,1)}), bf16[4,256,2048]{2,1,0:T(8,128)(2,1)}) %all-gather.3.cloned.1.call-update) | async-done | bytes 4194320 | tf_op jit(solution)/shard_map/all_gather | solution.py:121
  152.8 3.6 %fusion.11 = f32[1024,256]{1,0:T(8,128)S(1)} fusion(bf16[1024,2048]{1,0:T(8,128)(2,1)} %bitcast.80, bf16[1,2048,256]{2,1,0:T(8,128)(2,1)S(1)} %copy-done.8), kind=kOutput, calls=%fused_computation.23 | convolution fusion | flops 1073741824 | bytes 6291456 | tf_op jit(solution)/shard_map/dot_general | solution.py:123
  156.4 0.1 copy-done.9
  156.5 2.1 fusion.4
  158.6 23.0 %all-gather.5.cloned.1.call-done = bf16[1024,1024]{1,0:T(8,128)(2,1)} async-done(((bf16[1024,256]{1,0:T(8,128)(2,1)}), bf16[1024,1024]{1,0:T(8,128)(2,1)}) %all-gather.5.cloned.1.call-update) | async-done | bytes 2097168 | tf_op jit(solution)/shard_map/all_gather | solution.py:127
  181.6 3.9 %convolution_convert_fusion = bf16[1024,512]{1,0:T(8,128)(2,1)} fusion(bf16[1024,1024]{1,0:T(8,128)(2,1)} %all-gather.5.cloned.1.call-done, bf16[1,1024,512]{2,1,0:T(8,128)(2,1)S(1)} %copy-done.10), kind=kOutput, calls=%fused_computation.9 | convolution fusion | flops 1074266112 | bytes 4194304 | tf_op jit(solution)/shard_map/dot_general | solution.py:130
  185.5 4.7 %all-to-all-start.1 = ((bf16[4,256,512]{2,1,0:T(8,128)(2,1)}), bf16[4,256,512]{2,1,0:T(8,128)(2,1)S(1)}, u32[]{:S(2)}, u32[]{:S(2)}) async-start(bf16[4,256,512]{2,1,0:T(8,128)(2,1)} %bitcast.73), calls=%async_computation.1 | async-start | bytes 2097152 | tf_op jit(solution)/shard_map/all_to_all | solution.py:133
  190.3 2.1 fusion.42
  192.5 0.4 fusion.7
  192.9 7.5 %all_gather.9 = bf16[256,1024]{1,0:T(8,128)(2,1)} all-gather(bf16[256,256]{1,0:T(8,128)(2,1)S(1)} %fusion.7), channel_id=1, replica_groups=mesh['grp'=2,'sp'=4,'tp'=4] {'tp'}, dimensions={1}, use_global_device_ids=true | all-gather | bytes 655360 | tf_op jit(solution)/shard_map/all_gather | solution.py:128
  200.5 15.8 %all-to-all-done.1 = bf16[4,256,512]{2,1,0:T(8,128)(2,1)S(1)} async-done(((bf16[4,256,512]{2,1,0:T(8,128)(2,1)}), bf16[4,256,512]{2,1,0:T(8,128)(2,1)S(1)}, u32[]{:S(2)}, u32[]{:S(2)}) %all-to-all-start.1) | async-done | bytes 1048608 | tf_op jit(solution)/shard_map/all_to_all | solution.py:133
  216.3 2.6 %gather_fusion.1 = bf16[512,512]{1,0:T(8,128)(2,1)} fusion(bf16[1024,512]{1,0:T(8,128)(2,1)S(1)} %bitcast.71, s32[1024]{0:T(1024)S(1)} %pad_clamp_fusion), kind=kCustom, calls=%fused_computation.1 | custom fusion | bytes 1050624 | tf_op jit(solution)/shard_map/gather | solution.py:141
  218.9 1.7 reshape.184
  220.6 1.3 multiply_reduce_fusion
  222.0 2.5 %fusion.6 = bf16[256,512]{1,0:T(8,128)(2,1)} fusion(f32[256,512]{1,0:T(8,128)S(1)} %multiply_reduce_fusion, bf16[256,1024]{1,0:T(8,128)(2,1)} %all_gather.9, bf16[1024,512]{1,0:T(8,128)(2,1)} %param.31, bf16[256,2048]{1,0:T(8,128)(2,1)S(1)} %get-tuple-element.6, s32[]{:T(128)S(6)} %select_n.49), kind=kOutput, calls=%fused_computation.16 | convolution fusion | flops 268959744 | bytes 2621444 | tf_op jit(solution)/shard_map/dot_general | solution.py:143
  (59 shorter events, 1.5 us)
Async XLA Ops:
  6.5 24.1 %copy-start = (bf16[256,2048]{1,0:T(8,128)(2,1)S(1)}, bf16[256,2048]{1,0:T(8,128)(2,1)}, u32[]{:S(2)}) copy-start(bf16[256,2048]{1,0:T(8,128)(2,1)} %param.24) | copy-start | bytes 3145732
  6.5 75.6 %all-reduce.2.cloned.1.call-start = ((), (), s32[]{:S(2)}) async-start(), calls=%async_computation.2 | async-start | bytes 4194304 | tf_op jit(solution)/shard_map/psum | solution.py:92
  7.3 20.6 %collective-permute-start.1 = (bf16[128]{0:T(256)(128)(2,1)S(1)}, bf16[128]{0:T(256)(128)(2,1)S(1)}, u32[]{:S(2)}, u32[]{:S(2)}) collective-permute-start(bf16[128]{0:T(256)(128)(2,1)S(1)} %slice.47), channel_id=1, source_target_pairs={{0,4},{4,8},{8,12},{1,5},{5,9},{9,13},{2,6},{6,10},{10,14},{3,7},{... | collective-permute-start | bytes 776 | tf_op jit(solution)/shard_map/ppermute | solution.py:16
  13.1 15.0 %collective-permute-start.2 = (bf16[128,128]{1,0:T(8,128)(2,1)S(1)}, bf16[128,128]{1,0:T(8,128)(2,1)S(1)}, u32[]{:S(2)}, u32[]{:S(2)}) collective-permute-start(bf16[128,128]{1,0:T(8,128)(2,1)S(1)} %slice.50), channel_id=1, source_target_pairs={{0,4},{4,8},{8,12},{1,5},{5,9},{9,13},{2,6},{6,10},{10,14},{3,7},{... | collective-permute-start | bytes 98312 | tf_op jit(solution)/shard_map/ppermute | solution.py:16
  17.3 12.5 %collective-permute-start = (bf16[128,128]{1,0:T(8,128)(2,1)S(1)}, bf16[128,128]{1,0:T(8,128)(2,1)S(1)}, u32[]{:S(2)}, u32[]{:S(2)}) collective-permute-start(bf16[128,128]{1,0:T(8,128)(2,1)S(1)} %slice.45), channel_id=1, source_target_pairs={{0,4},{4,8},{8,12},{1,5},{5,9},{9,13},{2,6},{6,10},{10,14},{3,7},{... | collective-permute-start | bytes 98312 | tf_op jit(solution)/shard_map/ppermute | solution.py:16
  25.8 4.0 %copy-start.4 = (bf16[256,128]{1,0:T(8,128)(2,1)S(1)}, bf16[256,128]{1,0:T(8,128)(2,1)}, u32[]{:S(2)}) copy-start(bf16[256,128]{1,0:T(8,128)(2,1)} %param.19) | copy-start | bytes 196612
  32.4 49.8 %copy-start.3 = (bf16[256,2048]{1,0:T(8,128)(2,1)S(1)}, bf16[256,2048]{1,0:T(8,128)(2,1)}, u32[]{:S(2)}) copy-start(bf16[256,2048]{1,0:T(8,128)(2,1)} %param.16) | copy-start | bytes 3145732
  32.4 120.4 %all-gather.3.cloned.1.call-start = ((), (), s32[]{:S(2)}) async-start(), calls=%async_computation.3 | async-start | bytes 5242880 | tf_op jit(solution)/shard_map/all_gather | solution.py:121
  35.7 48.5 %copy-start.5 = (f32[2048]{0:T(1024)S(1)}, f32[2048]{0:T(1024)}, u32[]{:S(2)}) copy-start(f32[2048]{0:T(1024)} %param.25) | copy-start | bytes 24580
  84.5 1.0 copy-start.1
  89.6 63.1 %copy-start.8 = (bf16[1,2048,256]{2,1,0:T(8,128)(2,1)S(1)}, bf16[1,2048,256]{2,1,0:T(8,128)(2,1)}, u32[]{:S(2)}) copy-start(bf16[1,2048,256]{2,1,0:T(8,128)(2,1)} %param.26) | copy-start | bytes 3145732
  119.8 61.8 %all-gather.5.cloned.1.call-start = ((), (), s32[]{:S(2)}) async-start(), calls=%async_computation.4 | async-start | bytes 2621440 | tf_op jit(solution)/shard_map/all_gather | solution.py:127
  152.8 3.6 %copy-start.7 = (bf16[4,256,2048]{2,1,0:T(8,128)(2,1)S(1)}, bf16[4,256,2048]{2,1,0:T(8,128)(2,1)}, u32[]{:S(2)}) copy-start(bf16[4,256,2048]{2,1,0:T(8,128)(2,1)} %all-gather.3.cloned.1.call-done) | copy-start | bytes 12582916
  152.8 3.7 %copy-start.9 = (bf16[1,2048,256]{2,1,0:T(8,128)(2,1)S(1)}, bf16[1,2048,256]{2,1,0:T(8,128)(2,1)}, u32[]{:S(2)}) copy-start(bf16[1,2048,256]{2,1,0:T(8,128)(2,1)} %param.27) | copy-start | bytes 3145732
  156.5 25.1 %copy-start.10 = (bf16[1,1024,512]{2,1,0:T(8,128)(2,1)S(1)}, bf16[1,1024,512]{2,1,0:T(8,128)(2,1)}, u32[]{:S(2)}) copy-start(bf16[1,1024,512]{2,1,0:T(8,128)(2,1)} %param.28) | copy-start | bytes 3145732
  185.5 4.7 %copy-start.6 = (f32[256,2]{0,1:T(2,128)S(1)}, f32[256,2]{0,1:T(2,128)}, u32[]{:S(2)}) copy-start(f32[256,2]{0,1:T(2,128)} %param.22) | copy-start | bytes 6148
  185.5 30.8 %all-to-all-start.1 = ((bf16[4,256,512]{2,1,0:T(8,128)(2,1)}), bf16[4,256,512]{2,1,0:T(8,128)(2,1)S(1)}, u32[]{:S(2)}, u32[]{:S(2)}) async-start(bf16[4,256,512]{2,1,0:T(8,128)(2,1)} %bitcast.73), calls=%async_computation.1 | async-start | bytes 2097152 | tf_op jit(solution)/shard_map/all_to_all | solution.py:133
  190.3 2.2 copy-start.2
  190.3 2.2 copy-start.11
Sparse Core Ops, SparseCore 0:
  32.5 49.5 all-reduce.1
  119.9 32.7 all-gather.2
  158.8 22.8 all-gather.4
where the time goes:
time: 232 us; the launch traced here: 231 us
  waiting for transfers between devices  118 us (51%)
  blocking collectives  37.7 us (16%)
  local copies, waits for them, and re-layouts  19.6 us (8%)
  matrix products  17.1 us (7%)
  starting transfers between devices  16.7 us (7%)
  between operations  13.5 us (6%)
  other arithmetic  8.15 us (4%)
    psum x1, waiting for transfers between devices, shards(): summed = lax.psum(partial_value, 'tp')  46.5 us
    all_gather x1, waiting for transfers between devices, shards(): arrived = lax.all_gather(pieces, 'tp', axis=2, tiled=True)  32.9 us
    all_to_all x1, blocking collectives, shards(): lax.all_to_all(outgoing.reshape(experts, capacity, col_width), 'sp', spli...  30.1 us
    all_gather x1, waiting for transfers between devices, shards(): lax.all_gather(expert_act, 'tp', axis=1, tiled=True)  23 us
    all_to_all x1, waiting for transfers between devices, shards(): lax.all_to_all(expert_out.reshape(experts, capacity, col_width), 'sp', sp...  15.8 us
    ppermute x3, starting transfers between devices, passed_along(): lax.ppermute(value, axis, [(source, source + steps) for source in range(l...  11.9 us
    all_gather x1, blocking collectives, shards(): lax.all_gather(shared_act, 'tp', axis=1, tiled=True)  7.53 us
    all_to_all x1, starting transfers between devices, shards(): lax.all_to_all(expert_out.reshape(experts, capacity, col_width), 'sp', sp...  4.71 us
  transfers between devices with their start and end apart: 7, of which 4 were waited for; matrix products, arithmetic and copies ran while one was open for 7% of the time, Pallas kernels for 0%

commit v1 on v0

--- a/solution.py
+++ b/solution.py
@@ -1,6 +1,9 @@
+import functools
 import jax
 import jax.numpy as jnp
 from jax import lax
+from jax.experimental import pallas as pl
+from jax.experimental.pallas import tpu as pltpu
 from jax.sharding import PartitionSpec as P
 
 HEAD_DIM = 64
@@ -144,6 +147,533 @@
     return (updated_cols.astype(jnp.float32) + shared_cols + routed).astype(jnp.bfloat16)
 
 
+MESH = pl.DeviceIdType.MESH
+
+
+def fused_kernel(
+    dims,
+    res_hbm,
+    q_ref,
+    k_ref,
+    v_ref,
+    seg_row,
+    seg_col,
+    routes_ref,
+    rw_ref,
+    sinks_ref,
+    wo_hbm,
+    gain_ref,
+    eg_hbm,
+    eu_hbm,
+    ed_hbm,
+    sg_hbm,
+    su_hbm,
+    sd_hbm,
+    out_ref,
+    res_v,
+    wo_v,
+    gu_v,
+    sgu_v,
+    dn_v,
+    sdn_v,
+    kh,
+    vh,
+    mh,
+    att,
+    b1s,
+    b1r,
+    b2s,
+    b2r,
+    keep,
+    upd,
+    norm_v,
+    act,
+    eout,
+    eback,
+    acc,
+    w_sem,
+    halo_s,
+    halo_r,
+    b_s,
+    b_r,
+    u_s,
+    u_r,
+    a_s,
+    a_r,
+    e_s,
+    e_r,
+):
+    rows, cols, width, window, hidden, heads, group = dims
+    bf16, f32 = jnp.bfloat16, jnp.float32
+    s = lax.axis_index("sp")
+    t = lax.axis_index("tp")
+    core = t % 2
+    chip = t // 2
+    mate = t + 1 - 2 * core
+    over = t + 2 - 4 * chip
+    diag = 3 - t
+
+    def remote(src, dst, send, recv, sp, tp):
+        return pltpu.make_async_remote_copy(
+            src_ref=src,
+            dst_ref=dst,
+            send_sem=send,
+            recv_sem=recv,
+            device_id={"sp": sp, "tp": tp},
+            device_id_type=MESH,
+        )
+
+    own_cols = pl.ds(pl.multiple_of(t * cols, cols), cols)
+    loads = [
+        pltpu.make_async_copy(wo_hbm, wo_v, w_sem.at[0]),
+        pltpu.make_async_copy(res_hbm.at[:, own_cols], res_v, w_sem.at[1]),
+        pltpu.make_async_copy(eg_hbm.at[0], gu_v.at[:, pl.ds(0, hidden)], w_sem.at[2]),
+        pltpu.make_async_copy(eu_hbm.at[0], gu_v.at[:, pl.ds(hidden, hidden)], w_sem.at[3]),
+        pltpu.make_async_copy(sg_hbm, sgu_v.at[:, pl.ds(0, hidden)], w_sem.at[4]),
+        pltpu.make_async_copy(su_hbm, sgu_v.at[:, pl.ds(hidden, hidden)], w_sem.at[5]),
+        pltpu.make_async_copy(ed_hbm.at[0], dn_v, w_sem.at[6]),
+        pltpu.make_async_copy(sd_hbm, sdn_v, w_sem.at[7]),
+    ]
+    for load in loads:
+        load.start()
+
+    barrier = pltpu.get_barrier_semaphore()
+    pl.semaphore_signal(barrier, inc=1, device_id={"sp": s, "tp": mate}, device_id_type=MESH)
+    pl.semaphore_signal(barrier, inc=1, device_id={"sp": s, "tp": over}, device_id_type=MESH)
+    for step in range(1, 4):
+        pl.semaphore_signal(
+            barrier, inc=1, device_id={"sp": (s + step) % 4, "tp": t}, device_id_type=MESH
+        )
+    pl.semaphore_wait(barrier, 5)
+
+    tail = pl.ds(rows - window, window)
+    up_sp, down_sp = (s + 1) % 4, (s + 3) % 4
+    halos = [
+        remote(k_ref.at[tail], kh, halo_s.at[0], halo_r.at[0], up_sp, t),
+        remote(v_ref.at[tail], vh, halo_s.at[1], halo_r.at[1], up_sp, t),
+        remote(seg_row.at[:, tail], mh, halo_s.at[2], halo_r.at[2], up_sp, t),
+    ]
+
+    @pl.when(s < 3)
+    def _():
+        for copy in halos:
+            copy.start()
+
+    @pl.when(s == 0)
+    def _():
+        kh[...] = jnp.zeros_like(kh)
+        vh[...] = jnp.zeros_like(vh)
+        mh[...] = jnp.full(mh.shape, -1.0, f32)
+
+    q_pos = lax.broadcasted_iota(jnp.int32, (window, window), 0)
+    k_pos = lax.broadcasted_iota(jnp.int32, (window, window), 1)
+
+    def attend(n):
+        here = pl.ds(n * window, window)
+        if n == 0:
+            k_prev, v_prev, m_prev = kh[...], vh[...], mh[0:1, :]
+        else:
+            before = pl.ds((n - 1) * window, window)
+            k_prev, v_prev, m_prev = k_ref[before, :], v_ref[before, :], seg_row[0:1, before]
+        k_own, v_own, m_own = k_ref[here, :], v_ref[here, :], seg_row[0:1, here]
+        marks = seg_col[here, :]
+        ok_prev = (k_pos > q_pos) & (marks == m_prev)
+        ok_own = (k_pos <= q_pos) & (marks == m_own)
+        for h in range(heads):
+            kv = slice((h // group) * HEAD_DIM, (h // group + 1) * HEAD_DIM)
+            qh = q_ref[here, h * HEAD_DIM : (h + 1) * HEAD_DIM]
+            contract = (((1,), (1,)), ((), ()))
+            sc_prev = lax.dot_general(
+                qh, k_prev[:, kv], contract, preferred_element_type=f32
+            ) * HEAD_DIM ** (-0.5)
+            sc_own = lax.dot_general(
+                qh, k_own[:, kv], contract, preferred_element_type=f32
+            ) * HEAD_DIM ** (-0.5)
+            sc_prev = jnp.where(ok_prev, sc_prev, -jnp.inf)
+            sc_own = jnp.where(ok_own, sc_own, -jnp.inf)
+            sink = sinks_ref[h]
+            top = jnp.maximum(
+                jnp.max(jnp.maximum(sc_prev, sc_own), axis=-1, keepdims=True), sink
+            )
+            ex_prev = jnp.exp(sc_prev - top)
+            ex_own = jnp.exp(sc_own - top)
+            total = jnp.sum(ex_prev + ex_own, axis=-1, keepdims=True) + jnp.exp(sink - top)
+            p_prev = (ex_prev / total).astype(bf16)
+            p_own = (ex_own / total).astype(bf16)
+            got = jnp.dot(p_prev, v_prev[:, kv], preferred_element_type=f32) + jnp.dot(
+                p_own, v_own[:, kv], preferred_element_type=f32
+            )
+            att[here, h * HEAD_DIM : (h + 1) * HEAD_DIM] = got.astype(bf16)
+
+    def project(n, chunk):
+        where = pl.ds(pl.multiple_of(chunk * cols, cols), cols)
+        return jnp.dot(
+            att[pl.ds(n * window, window), :], wo_v[:, where], preferred_element_type=f32
+        )
+
+    halves = list(range(rows // window))[::-1]
+    pending = []
+    first = {}
+    for n in halves:
+        if n == 0:
+
+            @pl.when(s > 0)
+            def _():
+                for copy in halos:
+                    copy.wait_recv()
+
+        attend(n)
+        if n == halves[0]:
+            loads[0].wait()
+        for far in (1, 0):
+            chunk = (over if far else t) + 1 - 2 * core
+            b1s[n, far] = project(n, chunk).astype(bf16)
+            copy = remote(
+                b1s.at[n, far], b1r.at[n, far], b_s.at[n, far], b_r.at[n, far], s, mate
+            )
+            copy.start()
+            pending.append(copy)
+            first[n, far] = copy
+    second = {}
+    for n in halves:
+        mine = project(n, over)
+        first[n, 1].wait_recv()
+        b2s[n] = (mine + b1r[n, 1].astype(f32)).astype(bf16)
+        copy = remote(b2s.at[n], b2r.at[n], b_s.at[n, 2], b_r.at[n, 2], s, over)
+        copy.start()
+        pending.append(copy)
+        second[n] = copy
+    loads[1].wait()
+    for n in halves:
+        here = pl.ds(n * window, window)
+        mine = project(n, t) + res_v[here, :].astype(f32)
+        first[n, 0].wait_recv()
+        keep[here, :] = mine + b1r[n, 0].astype(f32)
+
+    def piece(b, chunk, n):
+        return upd.at[b, chunk, pl.ds(n * window, window)]
+
+    def share(kind, k, b, chunk, n, sp, tp):
+        return remote(
+            piece(b, chunk, n),
+            piece(b, chunk, n),
+            u_s.at[kind, k, n],
+            u_r.at[b, chunk, n],
+            sp,
+            tp,
+        )
+
+    conditional = []
+    for n in halves:
+        here = pl.ds(n * window, window)
+        second[n].wait_recv()
+        upd[s, t, here, :] = (keep[here, :] + b2r[n].astype(f32)).astype(bf16)
+        over_copy = share(3, 0, s, t, n, s, over)
+        over_copy.start()
+        up_copy = share(0, 0, s, t, n, up_sp, t)
+        down_copy = share(1, 0, s, t, n, down_sp, t)
+
+        @pl.when(s < 3)
+        def _():
+            up_copy.start()
+
+        @pl.when(s > 0)
+        def _():
+            down_copy.start()
+
+        mate_copy = share(2, 0, s, t, n, s, mate)
+        mate_copy.start()
+        pending += [over_copy, mate_copy]
+        conditional += [(s < 3, up_copy), (s > 0, down_copy)]
+
+    side = s // 2
+    edge = s + side * (3 - 2 * s)
+    order = [s]
+    for k in range(1, 4):
+        flat = k - edge if k == 1 else k
+        order.append(flat + side * (3 - 2 * flat))
+
+    def arrive(k):
+        b = order[k]
+        for n in halves:
+            share(0, k, b, t, n, s, mate).wait_recv()
+            copy = share(3, k, b, t, n, s, over)
+            copy.start()
+            to_up = share(0, k, b, t, n, up_sp, t)
+            to_down = share(1, k, b, t, n, down_sp, t)
+            rising = (b < s) & (s < 3)
+            falling = (b > s) & (s > 0)
+
+            @pl.when(rising)
+            def _():
+                to_up.start()
+
+            @pl.when(falling)
+            def _():
+                to_down.start()
+
+            conditional.extend([(rising, to_up), (falling, to_down)])
+            mate_copy = share(2, k, b, t, n, s, mate)
+            mate_copy.start()
+            pending.extend([copy, mate_copy])
+
+    def relay(k):
+        b = order[k]
+        for n in halves:
+            share(4, k, b, over, n, s, mate).wait_recv()
+            copy = share(4, k, b, over, n, s, mate)
+            copy.start()
+            pending.append(copy)
+
+    def normalize(k):
+        b = order[k]
+        for n in halves:
+            share(2, k, b, mate, n, s, mate).wait_recv()
+            share(4, k, b, diag, n, s, mate).wait_recv()
+        step = 32
+
+        def body(i, carry):
+            here = pl.ds(pl.multiple_of(i * step, step), step)
+            squares = jnp.zeros((step, 1), f32)
+            for chunk in range(4):
+                part = upd[b, chunk, here, :].astype(f32)
+                squares = squares + jnp.sum(part * part, axis=-1, keepdims=True)
+            inv = lax.rsqrt(squares / width + epsilon)
+            for chunk in range(4):
+                part = upd[b, chunk, here, :].astype(f32)
+                span = slice(chunk * cols, (chunk + 1) * cols)
+                norm_v[here, span] = (part * inv * gain_ref[0:1, span]).astype(bf16)
+            return carry
+
+        lax.fori_loop(0, rows // step, body, 0)
+
+    def pass_on(slot, kind, chunk, tp):
+        return remote(
+            act.at[slot, chunk],
+            act.at[slot, chunk],
+            a_s.at[kind, slot],
+            a_r.at[slot, chunk],
+            s,
+            tp,
+        )
+
+    def activate(slot, weight):
+        both = jnp.dot(norm_v[...], weight[...], preferred_element_type=f32)
+        gate, lin = both[:, :hidden], both[:, hidden:]
+        act[slot, t] = (gate / (1.0 + jnp.exp(-gate)) * lin).astype(bf16)
+        for kind, tp in ((0, over), (1, mate)):
+            copy = pass_on(slot, kind, t, tp)
+            copy.start()
+            pending.append(copy)
+
+    def relay_act(slot):
+        pass_on(slot, 2, over, mate).wait_recv()
+        copy = pass_on(slot, 2, over, mate)
+        copy.start()
+        pending.append(copy)
+
+    def contract_act(slot, weight):
+        pass_on(slot, 1, mate, mate).wait_recv()
+        pass_on(slot, 2, diag, mate).wait_recv()
+        total = None
+        for chunk in range(4):
+            part = jnp.dot(
+                act[slot, chunk],
+                weight[chunk * hidden : (chunk + 1) * hidden, :],
+                preferred_element_type=f32,
+            )
+            total = part if total is None else total + part
+        return total
+
+
+    def finish(k):
+        eout[k] = contract_act(k, dn_v).astype(bf16)
+        copy = remote(eout.at[k], eback.at[s], e_s.at[k], e_r.at[s], order[k], t)
+        copy.start()
+        pending.append(copy)
+
+    relay(0)
+    arrive(1)
+    loads[2].wait()
+    loads[3].wait()
+    normalize(0)
+    activate(0, gu_v)
+    loads[4].wait()
+    loads[5].wait()
+    activate(4, sgu_v)
+    relay(1)
+    arrive(2)
+    normalize(1)
+    activate(1, gu_v)
+    relay_act(0)
+    relay_act(4)
+    relay(2)
+    arrive(3)
+    normalize(2)
+    activate(2, gu_v)
+    relay_act(1)
+    relay(3)
+    loads[6].wait()
+    finish(1)
+    normalize(3)
+    activate(3, gu_v)
+    relay_act(2)
+    finish(2)
+    eout[0] = contract_act(0, dn_v).astype(bf16)
+    loads[7].wait()
+    acc[...] = contract_act(4, sdn_v)
+    relay_act(3)
+    finish(3)
+
+    def weight_of(e):
+        total = jnp.zeros((rows, 1), f32)
+        for k in range(routes_ref.shape[1]):
+            total = total + jnp.where(
+                routes_ref[:, k : k + 1] == e, rw_ref[:, k : k + 1], 0.0
+            )
+        return total
+
+    acc[...] = (
+        acc[...]
+        + upd[s, t].astype(f32)
+        + weight_of(s) * eout[0].astype(f32)
+    )
+    for k in range(1, 4):
+        b = order[k]
+        remote(eout.at[k], eback.at[b], e_s.at[k], e_r.at[b], b, t).wait_recv()
+        acc[...] = acc[...] + weight_of(b) * eback[b].astype(f32)
+    out_ref[...] = acc[...].astype(bf16)
+
+    for copy in pending:
+        copy.wait_send()
+    for when, copy in conditional:
+
+        @pl.when(when)
+        def _():
+            copy.wait_send()
+
+    @pl.when(s < 3)
+    def _():
+        for copy in halos:
+            copy.wait_send()
+
+
+def layer(
+    residual,
+    queries,
+    keys,
+    values,
+    segments,
+    routes,
+    route_weight,
+    sinks,
+    out_weight,
+    norm_gain,
+    expert_gate,
+    expert_up,
+    expert_down,
+    shared_gate,
+    shared_up,
+    shared_down,
+):
+    arguments = (
+        residual,
+        queries,
+        keys,
+        values,
+        segments,
+        routes,
+        route_weight,
+        sinks,
+        out_weight,
+        norm_gain,
+        expert_gate,
+        expert_up,
+        expert_down,
+        shared_gate,
+        shared_up,
+        shared_down,
+    )
+    rows, width = residual.shape
+    n_sp, n_tp = lax.axis_size("sp"), lax.axis_size("tp")
+    capacity = 2 * rows * routes.shape[1] // n_sp
+    hidden = expert_gate.shape[2]
+    if n_sp != 4 or n_tp != 4 or capacity < rows or shared_gate.shape[1] != hidden:
+        return shards(*arguments)
+    cols = width // n_tp
+    heads = queries.shape[1] // HEAD_DIM
+    group = queries.shape[1] // keys.shape[1]
+    kv_width = keys.shape[1]
+    blocks = rows // WINDOW
+    bf16, f32 = jnp.bfloat16, jnp.float32
+    marks = segments.astype(f32)
+    vmem = pl.BlockSpec(memory_space=pltpu.VMEM)
+    anywhere = pl.BlockSpec(memory_space=pl.ANY)
+    dma = pltpu.SemaphoreType.DMA
+    return pl.pallas_call(
+        functools.partial(fused_kernel, (rows, cols, width, WINDOW, hidden, heads, group)),
+        out_shape=jax.ShapeDtypeStruct((rows, cols), bf16),
+        in_specs=[anywhere]
+        + [vmem] * 7
+        + [pl.BlockSpec(memory_space=pltpu.SMEM), anywhere, vmem]
+        + [anywhere] * 6,
+        out_specs=vmem,
+        scratch_shapes=[
+            pltpu.VMEM((rows, cols), bf16),
+            pltpu.VMEM(out_weight.shape, bf16),
+            pltpu.VMEM((width, 2 * hidden), bf16),
+            pltpu.VMEM((width, 2 * hidden), bf16),
+            pltpu.VMEM(expert_down.shape[1:], bf16),
+            pltpu.VMEM(shared_down.shape, bf16),
+            pltpu.VMEM((WINDOW, kv_width), bf16),
+            pltpu.VMEM((WINDOW, kv_width), bf16),
+            pltpu.VMEM((8, WINDOW), f32),
+            pltpu.VMEM((rows, heads * HEAD_DIM), bf16),
+            pltpu.VMEM((blocks, 2, WINDOW, cols), bf16),
+            pltpu.VMEM((blocks, 2, WINDOW, cols), bf16),
+            pltpu.VMEM((blocks, WINDOW, cols), bf16),
+            pltpu.VMEM((blocks, WINDOW, cols), bf16),
+            pltpu.VMEM((rows, cols), f32),
+            pltpu.VMEM((4, 4, rows, cols), bf16),
+            pltpu.VMEM((rows, width), bf16),
+            pltpu.VMEM((5, 4, rows, hidden), bf16),
+            pltpu.VMEM((4, rows, cols), bf16),
+            pltpu.VMEM((4, rows, cols), bf16),
+            pltpu.VMEM((rows, cols), f32),
+            dma((8,)),
+            dma((3,)),
+            dma((3,)),
+            dma((blocks, 3)),
+            dma((blocks, 3)),
+            dma((5, 4, blocks)),
+            dma((4, 4, blocks)),
+            dma((3, 5)),
+            dma((5, 4)),
+            dma((4,)),
+            dma((4,)),
+        ],
+        compiler_params=pltpu.CompilerParams(collective_id=0, has_side_effects=True),
+    )(
+        residual,
+        queries,
+        keys,
+        values,
+        jnp.broadcast_to(marks[None, :], (8, rows)),
+        marks[:, None],
+        routes,
+        route_weight,
+        sinks,
+        out_weight,
+        norm_gain[None, :],
+        expert_gate,
+        expert_up,
+        expert_down,
+        shared_gate,
+        shared_up,
+        shared_down,
+    )
+
+
 def solution(mesh):
     placed = (
         P(("grp", "sp"), None),
@@ -164,5 +694,5 @@
         P(None, "tp"),
     )
     return jax.shard_map(
-        shards, mesh=mesh, in_specs=placed, out_specs=P(("grp", "sp"), "tp"), check_vma=False
-    )
+        layer, mesh=mesh, in_specs=placed, out_specs=P(("grp", "sp"), "tp"), check_vma=False
+    )

time: 232 us -> 87.9 us (0.38)
  waiting for transfers between devices: 118 us -> 0 us
  Pallas kernels: 0 us -> 82.4 us
  blocking collectives: 37.7 us -> 0 us
  matrix products: 17.1 us -> 0 us
  starting transfers between devices: 16.7 us -> 0 us
  local copies, waits for them, and re-layouts: 19.6 us -> 5.36 us
  between operations: 13.5 us -> 0.01 us
  other arithmetic: 8.15 us -> 0.01 us
    pallas_call x0 -> x1, Pallas kernels: none -> 82.4 us  [layer(): pl.pallas_call(functools.partial(fused_kernel, (rows, cols, width, WINDOW...]
    all_gather x2 -> x0, waiting for transfers between devices: 55.9 us -> none  [the longest x1 32.9 us: shards(): arrived = lax.all_gather(pieces, 'tp', axis=2, tiled=True)]
    psum x1 -> x0, waiting for transfers between devices: 46.5 us -> none  [shards(): summed = lax.psum(partial_value, 'tp')]
    all_to_all x1 -> x0, blocking collectives: 30.1 us -> none  [shards(): lax.all_to_all(outgoing.reshape(experts, capacity, col_width), 'sp', spli...]
    dot_general x9 -> x0, matrix products: 17.1 us -> none  [the longest x1 3.86 us: shards(): jnp.dot(gathered_expert, expert_down[0], preferred_element_type=jnp.float32)]
    all_to_all x1 -> x0, waiting for transfers between devices: 15.8 us -> none  [shards(): lax.all_to_all(expert_out.reshape(experts, capacity, col_width), 'sp', sp...]
    ppermute x3 -> x0, starting transfers between devices: 11.9 us -> none  [passed_along(): lax.ppermute(value, axis, [(source, source + steps) for source in range(l...]
    all_gather x1 -> x0, blocking collectives: 7.53 us -> none  [shards(): lax.all_gather(shared_act, 'tp', axis=1, tiled=True)]
  transfers between devices with their start and end apart: 7 -> 0, of which waited for: 4 -> 0; matrix products, arithmetic and copies ran while one was open for 7% -> 0% of each run, Pallas kernels for 0% -> 0%
where the time goes in v1:
time: 87.9 us; the launch traced here: 87.8 us
  Pallas kernels  82.4 us (94%)
  local copies, waits for them, and re-layouts  5.36 us (6%)
    pallas_call x1, Pallas kernels, layer(): pl.pallas_call(functools.partial(fused_kernel, (rows, cols, width, WINDOW...  82.4 us
    unnamed x9, local copies, waits for them, and re-layouts  3.97 us

profile of v1, /device:TPU:0, one launch (start us, length us, event | category | flops | bytes accessed | tf_op | source)
XLA Modules:
  0.0 87.8 jit_solution(9811532045583052481)
XLA Ops:
  0.0 0.0 copy-start.2
  0.0 0.7 copy-done.2
  0.7 0.6 broadcast_in_dim.12.seg_row
  1.3 0.0 copy-start
  1.3 0.8 copy.19.seg_col
  2.1 0.0 copy-done
  2.1 0.0 copy-start.1
  2.1 0.8 copy.20.routes_ref
  2.9 0.0 copy-done.1
  2.9 0.8 copy.21.rw_ref
  3.7 82.4 %shard_map.154 = bf16[256,512]{1,0:T(8,128)(2,1)} custom-call(bf16[256,2048]{1,0:T(8,128)(2,1)} %res_hbm.1, bf16[256,256]{1,0:T(8,128)(2,1)} %q_ref.1, bf16[256,128]{1,0:T(8,128)(2,1)} %k_ref.1, bf16[256,128]{1,0:T(8,128)(2,1)} %v_ref.1, f32[8,256]{1,0:T(8,128)} %broadcast_in_dim.12.seg_row, f32[256,1]{1,0:T(8,128)} %copy.19.seg_col, ...), custom_call_target="tpu_custom_call" | custom-call | tf_op jit(solution)/shard_map/pallas_call | solution.py:613
  86.1 1.7 %copy.23 = bf16[256,512]{1,0:T(8,128)(2,1)} copy(bf16[256,512]{1,0:T(8,128)(2,1)} %shard_map.154) | data formatting | bytes 524288
  (1 shorter events, 0.0 us)
Async XLA Ops:
  0.0 0.7 copy-start.2
  1.3 0.8 copy-start
  2.1 0.8 copy-start.1

commit v2 on v1

--- a/solution.py
+++ b/solution.py
@@ -156,8 +156,7 @@
     q_ref,
     k_ref,
     v_ref,
-    seg_row,
-    seg_col,
+    seg_ref,
     routes_ref,
     rw_ref,
     sinks_ref,
@@ -179,6 +178,9 @@
     kh,
     vh,
     mh,
+    marks_v,
+    aux_rows,
+    aux_ref,
     att,
     b1s,
     b1r,
@@ -237,6 +239,12 @@
     for load in loads:
         load.start()
 
+    top_count = routes_ref.shape[0]
+    aux_rows[...] = jnp.zeros_like(aux_rows)
+    aux_rows[0:1, :] = seg_ref[...].astype(f32)
+    aux_rows[1 : 1 + top_count, :] = routes_ref[...].astype(f32)
+    aux_rows[1 + top_count : 1 + 2 * top_count, :] = rw_ref[...]
+    marks_v[...] = jnp.broadcast_to(aux_rows[0:1, pl.ds(rows - window, window)], (8, window))
     barrier = pltpu.get_barrier_semaphore()
     pl.semaphore_signal(barrier, inc=1, device_id={"sp": s, "tp": mate}, device_id_type=MESH)
     pl.semaphore_signal(barrier, inc=1, device_id={"sp": s, "tp": over}, device_id_type=MESH)
@@ -246,12 +254,15 @@
         )
     pl.semaphore_wait(barrier, 5)
 
+    def marks_across(n):
+        return aux_rows[0:1, pl.ds(n * window, window)]
+
     tail = pl.ds(rows - window, window)
     up_sp, down_sp = (s + 1) % 4, (s + 3) % 4
     halos = [
         remote(k_ref.at[tail], kh, halo_s.at[0], halo_r.at[0], up_sp, t),
         remote(v_ref.at[tail], vh, halo_s.at[1], halo_r.at[1], up_sp, t),
-        remote(seg_row.at[:, tail], mh, halo_s.at[2], halo_r.at[2], up_sp, t),
+        remote(marks_v, mh, halo_s.at[2], halo_r.at[2], up_sp, t),
     ]
 
     @pl.when(s < 3)
@@ -264,6 +275,10 @@
         kh[...] = jnp.zeros_like(kh)
         vh[...] = jnp.zeros_like(vh)
         mh[...] = jnp.full(mh.shape, -1.0, f32)
+
+    for n in range(rows // window):
+        here = pl.ds(n * window, window)
+        aux_ref[here, :] = jnp.transpose(aux_rows[:, here])
 
     q_pos = lax.broadcasted_iota(jnp.int32, (window, window), 0)
     k_pos = lax.broadcasted_iota(jnp.int32, (window, window), 1)
@@ -274,9 +289,9 @@
             k_prev, v_prev, m_prev = kh[...], vh[...], mh[0:1, :]
         else:
             before = pl.ds((n - 1) * window, window)
-            k_prev, v_prev, m_prev = k_ref[before, :], v_ref[before, :], seg_row[0:1, before]
-        k_own, v_own, m_own = k_ref[here, :], v_ref[here, :], seg_row[0:1, here]
-        marks = seg_col[here, :]
+            k_prev, v_prev, m_prev = k_ref[before, :], v_ref[before, :], marks_across(n - 1)
+        k_own, v_own, m_own = k_ref[here, :], v_ref[here, :], marks_across(n)
+        marks = aux_ref[here, 0:1]
         ok_prev = (k_pos > q_pos) & (marks == m_prev)
         ok_own = (k_pos <= q_pos) & (marks == m_own)
         for h in range(heads):
@@ -390,7 +405,7 @@
     edge = s + side * (3 - 2 * s)
     order = [s]
     for k in range(1, 4):
-        flat = k - edge if k == 1 else k
+        flat = (k, k + edge, k - 2 * edge, k)[k]
         order.append(flat + side * (3 - 2 * flat))
 
     def arrive(k):
@@ -492,45 +507,45 @@
         copy.start()
         pending.append(copy)
 
+    arrive(1)
     relay(0)
-    arrive(1)
+    arrive(2)
+    relay(1)
     loads[2].wait()
     loads[3].wait()
+    normalize(1)
+    activate(1, gu_v)
+    arrive(3)
+    relay(2)
+    normalize(2)
+    activate(2, gu_v)
+    relay_act(1)
+    loads[6].wait()
+    finish(1)
+    relay(3)
+    normalize(3)
+    activate(3, gu_v)
+    relay_act(2)
+    finish(2)
     normalize(0)
     activate(0, gu_v)
     loads[4].wait()
     loads[5].wait()
     activate(4, sgu_v)
-    relay(1)
-    arrive(2)
-    normalize(1)
-    activate(1, gu_v)
+    relay_act(3)
+    finish(3)
     relay_act(0)
     relay_act(4)
-    relay(2)
-    arrive(3)
-    normalize(2)
-    activate(2, gu_v)
-    relay_act(1)
-    relay(3)
-    loads[6].wait()
-    finish(1)
-    normalize(3)
-    activate(3, gu_v)
-    relay_act(2)
-    finish(2)
     eout[0] = contract_act(0, dn_v).astype(bf16)
     loads[7].wait()
     acc[...] = contract_act(4, sdn_v)
-    relay_act(3)
-    finish(3)
 
     def weight_of(e):
         total = jnp.zeros((rows, 1), f32)
-        for k in range(routes_ref.shape[1]):
-            total = total + jnp.where(
-                routes_ref[:, k : k + 1] == e, rw_ref[:, k : k + 1], 0.0
-            )
+        for k in range(1, top_count + 1):
+            weight = aux_ref[:, top_count + k : top_count + k + 1]
+            named = aux_ref[:, k : k + 1] == jnp.full((rows, 1), e, jnp.int32).astype(f32)
+            total = total + jnp.where(named, weight, 0.0)
         return total
 
     acc[...] = (
@@ -606,7 +621,6 @@
     kv_width = keys.shape[1]
     blocks = rows // WINDOW
     bf16, f32 = jnp.bfloat16, jnp.float32
-    marks = segments.astype(f32)
     vmem = pl.BlockSpec(memory_space=pltpu.VMEM)
     anywhere = pl.BlockSpec(memory_space=pl.ANY)
     dma = pltpu.SemaphoreType.DMA
@@ -614,7 +628,7 @@
         functools.partial(fused_kernel, (rows, cols, width, WINDOW, hidden, heads, group)),
         out_shape=jax.ShapeDtypeStruct((rows, cols), bf16),
         in_specs=[anywhere]
-        + [vmem] * 7
+        + [vmem] * 6
         + [pl.BlockSpec(memory_space=pltpu.SMEM), anywhere, vmem]
         + [anywhere] * 6,
         out_specs=vmem,
@@ -628,6 +642,9 @@
             pltpu.VMEM((WINDOW, kv_width), bf16),
             pltpu.VMEM((WINDOW, kv_width), bf16),
             pltpu.VMEM((8, WINDOW), f32),
+            pltpu.VMEM((8, WINDOW), f32),
+            pltpu.VMEM((WINDOW, rows), f32),
+            pltpu.VMEM((rows, WINDOW), f32),
             pltpu.VMEM((rows, heads * HEAD_DIM), bf16),
             pltpu.VMEM((blocks, 2, WINDOW, cols), bf16),
             pltpu.VMEM((blocks, 2, WINDOW, cols), bf16),
@@ -658,10 +675,9 @@
         queries,
         keys,
         values,
-        jnp.broadcast_to(marks[None, :], (8, rows)),
-        marks[:, None],
-        routes,
-        route_weight,
+        segments[None, :],
+        routes.T,
+        route_weight.T,
         sinks,
         out_weight,
         norm_gain[None, :],

time: 87.9 us -> 75.2 us (0.86)
  Pallas kernels: 82.4 us -> 73.3 us
  local copies, waits for them, and re-layouts: 5.36 us -> 1.67 us
    pallas_call x1, Pallas kernels: 82.4 us -> 73.3 us  [layer(): pl.pallas_call(functools.partial(fused_kernel, (rows, cols, width, WINDOW...]
    unnamed x9 -> x1, local copies, waits for them, and re-layouts: 3.97 us -> 1.67 us
    broadcast_in_dim x2 -> x0, local copies, waits for them, and re-layouts: 1.4 us -> none  [the longest x1 0.8 us: layer(): marks[:, None]]
where the time goes in v2:
time: 75.2 us; the launch traced here: 75 us
  Pallas kernels  73.3 us (97%)
  local copies, waits for them, and re-layouts  1.67 us (2%)
    pallas_call x1, Pallas kernels, layer(): pl.pallas_call(functools.partial(fused_kernel, (rows, cols, width, WINDOW...  73.3 us
    unnamed x1, local copies, waits for them, and re-layouts  1.67 us

profile of v2, /device:TPU:0, one launch (start us, length us, event | category | flops | bytes accessed | tf_op | source)
XLA Modules:
  0.0 75.0 jit_solution(5679468718705329315)
XLA Ops:
  0.0 73.3 %shard_map.154 = bf16[256,512]{1,0:T(8,128)(2,1)} custom-call(bf16[256,2048]{1,0:T(8,128)(2,1)} %res_hbm.1, bf16[256,256]{1,0:T(8,128)(2,1)} %q_ref.1, bf16[256,128]{1,0:T(8,128)(2,1)} %k_ref.1, bf16[256,128]{1,0:T(8,128)(2,1)} %v_ref.1, s32[1,256]{1,0:T(1,128)} %bitcast.7, s32[2,256]{1,0:T(2,128)} %bitcast.5, f32[2,256]{1,0:T(2,128)} %bitcast.6, ...), custom_call_target="tpu_custom_call" | custom-call | tf_op jit(solution)/shard_map/pallas_call | solution.py:627
  73.4 1.7 %copy.18 = bf16[256,512]{1,0:T(8,128)(2,1)} copy(bf16[256,512]{1,0:T(8,128)(2,1)} %shard_map.154) | data formatting | bytes 524288

commit v3 on v2

--- a/solution.py
+++ b/solution.py
@@ -408,37 +408,55 @@
         flat = (k, k + edge, k - 2 * edge, k)[k]
         order.append(flat + side * (3 - 2 * flat))
 
+    along = halves[:1]
+
+    def onward(k, kinds, chunk, n):
+        b = order[k]
+        to_up = share(kinds[0], k, b, chunk, n, up_sp, t)
+        to_down = share(kinds[1], k, b, chunk, n, down_sp, t)
+        rising = s < 3 if k == 0 else (b < s) & (s < 3)
+        falling = s > 0 if k == 0 else (b > s) & (s > 0)
+
+        @pl.when(rising)
+        def _():
+            to_up.start()
+
+        @pl.when(falling)
+        def _():
+            to_down.start()
+
+        conditional.extend([(rising, to_up), (falling, to_down)])
+
     def arrive(k):
         b = order[k]
         for n in halves:
             share(0, k, b, t, n, s, mate).wait_recv()
-            copy = share(3, k, b, t, n, s, over)
-            copy.start()
-            to_up = share(0, k, b, t, n, up_sp, t)
-            to_down = share(1, k, b, t, n, down_sp, t)
-            rising = (b < s) & (s < 3)
-            falling = (b > s) & (s > 0)
-
-            @pl.when(rising)
-            def _():
-                to_up.start()
-
-            @pl.when(falling)
-            def _():
-                to_down.start()
-
-            conditional.extend([(rising, to_up), (falling, to_down)])
+            onward(k, (0, 1), t, n)
+            if n not in along:
+                copy = share(3, k, b, t, n, s, over)
+                copy.start()
+                pending.append(copy)
             mate_copy = share(2, k, b, t, n, s, mate)
             mate_copy.start()
-            pending.extend([copy, mate_copy])
+            pending.append(mate_copy)
+
+    def relay_half(k, n):
+        b = order[k]
+        share(4, k, b, over, n, s, mate).wait_recv()
+        if n in along:
+            onward(k, (5, 6), over, n)
+        copy = share(4, k, b, over, n, s, mate)
+        copy.start()
+        pending.append(copy)
 
     def relay(k):
-        b = order[k]
         for n in halves:
-            share(4, k, b, over, n, s, mate).wait_recv()
-            copy = share(4, k, b, over, n, s, mate)
-            copy.start()
-            pending.append(copy)
+            if k == 0 or n not in along:
+                relay_half(k, n)
+
+    def arrive_over(k):
+        for n in along:
+            relay_half(k, n)
 
     def normalize(k):
         b = order[k]
@@ -510,18 +528,21 @@
     arrive(1)
     relay(0)
     arrive(2)
+    arrive_over(1)
     relay(1)
     loads[2].wait()
     loads[3].wait()
     normalize(1)
     activate(1, gu_v)
     arrive(3)
+    arrive_over(2)
     relay(2)
     normalize(2)
     activate(2, gu_v)
     relay_act(1)
     loads[6].wait()
     finish(1)
+    arrive_over(3)
     relay(3)
     normalize(3)
     activate(3, gu_v)
@@ -662,7 +683,7 @@
             dma((3,)),
             dma((blocks, 3)),
             dma((blocks, 3)),
-            dma((5, 4, blocks)),
+            dma((7, 4, blocks)),
             dma((4, 4, blocks)),
             dma((3, 5)),
             dma((5, 4)),

time: 75.2 us -> 71.6 us (0.952)
  Pallas kernels: 73.3 us -> 69.8 us
    pallas_call x1, Pallas kernels: 73.3 us -> 69.8 us  [layer(): pl.pallas_call(functools.partial(fused_kernel, (rows, cols, width, WINDOW...]
where the time goes in v3:
time: 71.6 us; the launch traced here: 71.4 us
  Pallas kernels  69.8 us (97%)
  local copies, waits for them, and re-layouts  1.67 us (2%)
    pallas_call x1, Pallas kernels, layer(): pl.pallas_call(functools.partial(fused_kernel, (rows, cols, width, WINDOW...  69.8 us
    unnamed x1, local copies, waits for them, and re-layouts  1.67 us

profile of v3, /device:TPU:0, one launch (start us, length us, event | category | flops | bytes accessed | tf_op | source)
XLA Modules:
  0.0 71.4 jit_solution(8480593147113363626)
XLA Ops:
  0.0 69.8 %shard_map.154 = bf16[256,512]{1,0:T(8,128)(2,1)} custom-call(bf16[256,2048]{1,0:T(8,128)(2,1)} %res_hbm.1, bf16[256,256]{1,0:T(8,128)(2,1)} %q_ref.1, bf16[256,128]{1,0:T(8,128)(2,1)} %k_ref.1, bf16[256,128]{1,0:T(8,128)(2,1)} %v_ref.1, s32[1,256]{1,0:T(1,128)} %bitcast.7, s32[2,256]{1,0:T(2,128)} %bitcast.5, f32[2,256]{1,0:T(2,128)} %bitcast.6, ...), custom_call_target="tpu_custom_call" | custom-call | tf_op jit(solution)/shard_map/pallas_call | solution.py:648
  69.8 1.7 %copy.18 = bf16[256,512]{1,0:T(8,128)(2,1)} copy(bf16[256,512]{1,0:T(8,128)(2,1)} %shard_map.154) | data formatting | bytes 524288

commit v4 on v3

--- a/solution.py
+++ b/solution.py
@@ -148,6 +148,8 @@
 
 
 MESH = pl.DeviceIdType.MESH
+PARTS = 4
+ALONG = 1
 
 
 def fused_kernel(
@@ -313,8 +315,9 @@
             ex_prev = jnp.exp(sc_prev - top)
             ex_own = jnp.exp(sc_own - top)
             total = jnp.sum(ex_prev + ex_own, axis=-1, keepdims=True) + jnp.exp(sink - top)
-            p_prev = (ex_prev / total).astype(bf16)
-            p_own = (ex_own / total).astype(bf16)
+            inverse = 1.0 / total
+            p_prev = (ex_prev * inverse).astype(bf16)
+            p_own = (ex_own * inverse).astype(bf16)
             got = jnp.dot(p_prev, v_prev[:, kv], preferred_element_type=f32) + jnp.dot(
                 p_own, v_own[:, kv], preferred_element_type=f32
             )
@@ -365,8 +368,16 @@
         first[n, 0].wait_recv()
         keep[here, :] = mine + b1r[n, 0].astype(f32)
 
+    parts = u_s.shape[2]
+    part_rows = rows // parts
+    per_half = window // part_rows
+    listed = [n * per_half + i for n in halves for i in range(per_half)]
+
+    def of_half(n):
+        return [p for p in listed if n is None or p // per_half == n]
+
     def piece(b, chunk, n):
-        return upd.at[b, chunk, pl.ds(n * window, window)]
+        return upd.at[b, chunk, pl.ds(n * part_rows, part_rows)]
 
     def share(kind, k, b, chunk, n, sp, tp):
         return remote(
@@ -383,23 +394,24 @@
         here = pl.ds(n * window, window)
         second[n].wait_recv()
         upd[s, t, here, :] = (keep[here, :] + b2r[n].astype(f32)).astype(bf16)
-        over_copy = share(3, 0, s, t, n, s, over)
-        over_copy.start()
-        up_copy = share(0, 0, s, t, n, up_sp, t)
-        down_copy = share(1, 0, s, t, n, down_sp, t)
-
-        @pl.when(s < 3)
-        def _():
-            up_copy.start()
-
-        @pl.when(s > 0)
-        def _():
-            down_copy.start()
-
-        mate_copy = share(2, 0, s, t, n, s, mate)
-        mate_copy.start()
-        pending += [over_copy, mate_copy]
-        conditional += [(s < 3, up_copy), (s > 0, down_copy)]
+        for p in of_half(n):
+            over_copy = share(3, 0, s, t, p, s, over)
+            over_copy.start()
+            up_copy = share(0, 0, s, t, p, up_sp, t)
+            down_copy = share(1, 0, s, t, p, down_sp, t)
+
+            @pl.when(s < 3)
+            def _(up_copy=up_copy):
+                up_copy.start()
+
+            @pl.when(s > 0)
+            def _(down_copy=down_copy):
+                down_copy.start()
+
+            mate_copy = share(2, 0, s, t, p, s, mate)
+            mate_copy.start()
+            pending += [over_copy, mate_copy]
+            conditional += [(s < 3, up_copy), (s > 0, down_copy)]
 
     side = s // 2
     edge = s + side * (3 - 2 * s)
@@ -408,7 +420,7 @@
         flat = (k, k + edge, k - 2 * edge, k)[k]
         order.append(flat + side * (3 - 2 * flat))
 
-    along = halves[:1]
+    along = listed[:ALONG]
 
     def onward(k, kinds, chunk, n):
         b = order[k]
@@ -427,9 +439,9 @@
 
         conditional.extend([(rising, to_up), (falling, to_down)])
 
-    def arrive(k):
+    def arrive(k, half=None):
         b = order[k]
-        for n in halves:
+        for n in of_half(half):
             share(0, k, b, t, n, s, mate).wait_recv()
             onward(k, (0, 1), t, n)
             if n not in along:
@@ -449,8 +461,8 @@
         copy.start()
         pending.append(copy)
 
-    def relay(k):
-        for n in halves:
+    def relay(k, half=None):
+        for n in of_half(half):
             if k == 0 or n not in along:
                 relay_half(k, n)
 
@@ -458,15 +470,15 @@
         for n in along:
             relay_half(k, n)
 
-    def normalize(k):
+    def normalize(k, half):
         b = order[k]
-        for n in halves:
+        for n in of_half(half):
             share(2, k, b, mate, n, s, mate).wait_recv()
             share(4, k, b, diag, n, s, mate).wait_recv()
         step = 32
 
         def body(i, carry):
-            here = pl.ds(pl.multiple_of(i * step, step), step)
+            here = pl.ds(pl.multiple_of(half * window + i * step, step), step)
             squares = jnp.zeros((step, 1), f32)
             for chunk in range(4):
                 part = upd[b, chunk, here, :].astype(f32)
@@ -478,53 +490,65 @@
                 norm_v[here, span] = (part * inv * gain_ref[0:1, span]).astype(bf16)
             return carry
 
-        lax.fori_loop(0, rows // step, body, 0)
-
-    def pass_on(slot, kind, chunk, tp):
+        lax.fori_loop(0, window // step, body, 0)
+
+    def pass_on(slot, kind, chunk, tp, half):
+        place = act.at[slot, chunk, pl.ds(half * window, window)]
         return remote(
-            act.at[slot, chunk],
-            act.at[slot, chunk],
-            a_s.at[kind, slot],
-            a_r.at[slot, chunk],
-            s,
-            tp,
+            place, place, a_s.at[kind, slot, half], a_r.at[slot, chunk, half], s, tp
         )
 
-    def activate(slot, weight):
-        both = jnp.dot(norm_v[...], weight[...], preferred_element_type=f32)
+    def activate(slot, weight, half):
+        here = pl.ds(half * window, window)
+        both = jnp.dot(norm_v[here, :], weight[...], preferred_element_type=f32)
         gate, lin = both[:, :hidden], both[:, hidden:]
-        act[slot, t] = (gate / (1.0 + jnp.exp(-gate)) * lin).astype(bf16)
+        act[slot, t, here, :] = (gate / (1.0 + jnp.exp(-gate)) * lin).astype(bf16)
         for kind, tp in ((0, over), (1, mate)):
-            copy = pass_on(slot, kind, t, tp)
+            copy = pass_on(slot, kind, t, tp, half)
             copy.start()
             pending.append(copy)
 
-    def relay_act(slot):
-        pass_on(slot, 2, over, mate).wait_recv()
-        copy = pass_on(slot, 2, over, mate)
+    def relay_act(slot, half):
+        pass_on(slot, 2, over, mate, half).wait_recv()
+        copy = pass_on(slot, 2, over, mate, half)
         copy.start()
         pending.append(copy)
 
-    def contract_act(slot, weight):
-        pass_on(slot, 1, mate, mate).wait_recv()
-        pass_on(slot, 2, diag, mate).wait_recv()
+    def contract_act(slot, weight, half):
+        pass_on(slot, 1, mate, mate, half).wait_recv()
+        pass_on(slot, 2, diag, mate, half).wait_recv()
         total = None
         for chunk in range(4):
             part = jnp.dot(
-                act[slot, chunk],
+                act[slot, chunk, pl.ds(half * window, window), :],
                 weight[chunk * hidden : (chunk + 1) * hidden, :],
                 preferred_element_type=f32,
             )
             total = part if total is None else total + part
         return total
 
-
-    def finish(k):
-        eout[k] = contract_act(k, dn_v).astype(bf16)
-        copy = remote(eout.at[k], eback.at[s], e_s.at[k], e_r.at[s], order[k], t)
+    def give_back(k, b, half):
+        here = pl.ds(half * window, window)
+        return remote(
+            eout.at[k, here], eback.at[b, here], e_s.at[k, half], e_r.at[b, half], order[k], t
+        )
+
+    def finish(k, half):
+        here = pl.ds(half * window, window)
+        eout[k, here, :] = contract_act(k, dn_v, half).astype(bf16)
+        copy = give_back(k, s, half)
         copy.start()
         pending.append(copy)
 
+    def expert(k, half):
+        normalize(k, half)
+        activate(k, gu_v, half)
+
+    def each(step, *given):
+        for n in halves:
+            step(*given, n)
+
+    early, late = halves[0], halves[-1]
     arrive(1)
     relay(0)
     arrive(2)
@@ -532,34 +556,38 @@
     relay(1)
     loads[2].wait()
     loads[3].wait()
-    normalize(1)
-    activate(1, gu_v)
-    arrive(3)
+    each(expert, 1)
+    arrive(3, early)
     arrive_over(2)
-    relay(2)
-    normalize(2)
-    activate(2, gu_v)
-    relay_act(1)
-    loads[6].wait()
-    finish(1)
-    arrive_over(3)
-    relay(3)
-    normalize(3)
-    activate(3, gu_v)
-    relay_act(2)
-    finish(2)
-    normalize(0)
-    activate(0, gu_v)
+    each(expert, 0)
     loads[4].wait()
     loads[5].wait()
-    activate(4, sgu_v)
-    relay_act(3)
-    finish(3)
-    relay_act(0)
-    relay_act(4)
-    eout[0] = contract_act(0, dn_v).astype(bf16)
+    each(activate, 4, sgu_v)
+    relay(2)
+    each(expert, 2)
+    each(relay_act, 1)
+    loads[6].wait()
+    each(finish, 1)
+    arrive(3, late)
+    arrive_over(3)
+    each(relay_act, 0)
+    each(relay_act, 4)
+    relay(3, early)
+    expert(3, early)
+    each(relay_act, 2)
+    each(finish, 2)
+    relay(3, late)
+    expert(3, late)
+    for n in halves:
+        eout[0, pl.ds(n * window, window), :] = contract_act(0, dn_v, n).astype(bf16)
+    relay_act(3, early)
+    finish(3, early)
     loads[7].wait()
-    acc[...] = contract_act(4, sdn_v)
+    for n in halves:
+        here = pl.ds(n * window, window)
+        acc[here, :] = contract_act(4, sdn_v, n)
+    relay_act(3, late)
+    finish(3, late)
 
     def weight_of(e):
         total = jnp.zeros((rows, 1), f32)
@@ -569,16 +597,23 @@
             total = total + jnp.where(named, weight, 0.0)
         return total
 
-    acc[...] = (
-        acc[...]
-        + upd[s, t].astype(f32)
-        + weight_of(s) * eout[0].astype(f32)
-    )
+    weights = [weight_of(order[k]) for k in range(4)]
+    for n in halves:
+        here = pl.ds(n * window, window)
+        acc[here, :] = (
+            acc[here, :]
+            + upd[s, t, here, :].astype(f32)
+            + weights[0][n * window : (n + 1) * window] * eout[0, here, :].astype(f32)
+        )
     for k in range(1, 4):
-        b = order[k]
-        remote(eout.at[k], eback.at[b], e_s.at[k], e_r.at[b], b, t).wait_recv()
-        acc[...] = acc[...] + weight_of(b) * eback[b].astype(f32)
-    out_ref[...] = acc[...].astype(bf16)
+        for n in halves:
+            here = pl.ds(n * window, window)
+            give_back(k, order[k], n).wait_recv()
+            more = weights[k][n * window : (n + 1) * window] * eback[order[k], here, :].astype(f32)
+            if k < 3:
+                acc[here, :] = acc[here, :] + more
+            else:
+                out_ref[here, :] = (acc[here, :] + more).astype(bf16)
 
     for copy in pending:
         copy.wait_send()
@@ -683,12 +718,12 @@
             dma((3,)),
             dma((blocks, 3)),
             dma((blocks, 3)),
-            dma((7, 4, blocks)),
-            dma((4, 4, blocks)),
-            dma((3, 5)),
-            dma((5, 4)),
-            dma((4,)),
-            dma((4,)),
+            dma((7, 4, PARTS)),
+            dma((4, 4, PARTS)),
+            dma((3, 5, blocks)),
+            dma((5, 4, blocks)),
+            dma((4, blocks)),
+            dma((4, blocks)),
         ],
         compiler_params=pltpu.CompilerParams(collective_id=0, has_side_effects=True),
     )(

time: 71.6 us -> 74 us (1.034)
  Pallas kernels: 69.8 us -> 72.2 us
    pallas_call x1, Pallas kernels: 69.8 us -> 72.2 us  [layer(): pl.pallas_call(functools.partial(fused_kernel, (rows, cols, width, WINDOW...]
where the time goes in v4:
time: 74 us; the launch traced here: 73.9 us
  Pallas kernels  72.2 us (98%)
  local copies, waits for them, and re-layouts  1.67 us (2%)
    pallas_call x1, Pallas kernels, layer(): pl.pallas_call(functools.partial(fused_kernel, (rows, cols, width, WINDOW...  72.2 us
    unnamed x1, local copies, waits for them, and re-layouts  1.67 us

profile of v4, /device:TPU:0, one launch (start us, length us, event | category | flops | bytes accessed | tf_op | source)
XLA Modules:
  0.0 73.9 jit_solution(10972153428515881093)
XLA Ops:
  0.0 72.2 %shard_map.154 = bf16[256,512]{1,0:T(8,128)(2,1)} custom-call(bf16[256,2048]{1,0:T(8,128)(2,1)} %res_hbm.1, bf16[256,256]{1,0:T(8,128)(2,1)} %q_ref.1, bf16[256,128]{1,0:T(8,128)(2,1)} %k_ref.1, bf16[256,128]{1,0:T(8,128)(2,1)} %v_ref.1, s32[1,256]{1,0:T(1,128)} %bitcast.7, s32[2,256]{1,0:T(2,128)} %bitcast.5, f32[2,256]{1,0:T(2,128)} %bitcast.6, ...), custom_call_target="tpu_custom_call" | custom-call | tf_op jit(solution)/shard_map/pallas_call | solution.py:683
  72.2 1.7 %copy.18 = bf16[256,512]{1,0:T(8,128)(2,1)} copy(bf16[256,512]{1,0:T(8,128)(2,1)} %shard_map.154) | data formatting | bytes 524288

commit v5 on v4

--- a/solution.py
+++ b/solution.py
@@ -238,7 +238,7 @@
         pltpu.make_async_copy(ed_hbm.at[0], dn_v, w_sem.at[6]),
         pltpu.make_async_copy(sd_hbm, sdn_v, w_sem.at[7]),
     ]
-    for load in loads:
+    for load in loads[:2]:
         load.start()
 
     top_count = routes_ref.shape[0]
@@ -332,6 +332,7 @@
     halves = list(range(rows // window))[::-1]
     pending = []
     first = {}
+    second = {}
     for n in halves:
         if n == 0:
 
@@ -343,6 +344,8 @@
         attend(n)
         if n == halves[0]:
             loads[0].wait()
+            for load in loads[2:]:
+                load.start()
         for far in (1, 0):
             chunk = (over if far else t) + 1 - 2 * core
             b1s[n, far] = project(n, chunk).astype(bf16)
@@ -352,8 +355,6 @@
             copy.start()
             pending.append(copy)
             first[n, far] = copy
-    second = {}
-    for n in halves:
         mine = project(n, over)
         first[n, 1].wait_recv()
         b2s[n] = (mine + b1r[n, 1].astype(f32)).astype(bf16)
@@ -470,15 +471,21 @@
         for n in along:
             relay_half(k, n)
 
-    def normalize(k, half):
+    def span_of(half):
+        if half is None:
+            return halves, 0, rows
+        return [half], half * window, window
+
+    def normalize(k, half=None):
         b = order[k]
+        _, begin, length = span_of(half)
         for n in of_half(half):
             share(2, k, b, mate, n, s, mate).wait_recv()
             share(4, k, b, diag, n, s, mate).wait_recv()
         step = 32
 
         def body(i, carry):
-            here = pl.ds(pl.multiple_of(half * window + i * step, step), step)
+            here = pl.ds(pl.multiple_of(begin + i * step, step), step)
             squares = jnp.zeros((step, 1), f32)
             for chunk in range(4):
                 part = upd[b, chunk, here, :].astype(f32)
@@ -490,7 +497,7 @@
                 norm_v[here, span] = (part * inv * gain_ref[0:1, span]).astype(bf16)
             return carry
 
-        lax.fori_loop(0, window // step, body, 0)
+        lax.fori_loop(0, length // step, body, 0)
 
     def pass_on(slot, kind, chunk, tp, half):
         place = act.at[slot, chunk, pl.ds(half * window, window)]
@@ -498,29 +505,36 @@
             place, place, a_s.at[kind, slot, half], a_r.at[slot, chunk, half], s, tp
         )
 
-    def activate(slot, weight, half):
-        here = pl.ds(half * window, window)
+    def activate(slot, weight, half=None):
+        _, begin, length = span_of(half)
+        here = pl.ds(begin, length)
         both = jnp.dot(norm_v[here, :], weight[...], preferred_element_type=f32)
         gate, lin = both[:, :hidden], both[:, hidden:]
         act[slot, t, here, :] = (gate / (1.0 + jnp.exp(-gate)) * lin).astype(bf16)
-        for kind, tp in ((0, over), (1, mate)):
-            copy = pass_on(slot, kind, t, tp, half)
+
+    def ship(slot, half=None):
+        for n in span_of(half)[0]:
+            for kind, tp in ((0, over), (1, mate)):
+                copy = pass_on(slot, kind, t, tp, n)
+                copy.start()
+                pending.append(copy)
+
+    def relay_act(slot, half=None):
+        for n in span_of(half)[0]:
+            pass_on(slot, 2, over, mate, n).wait_recv()
+            copy = pass_on(slot, 2, over, mate, n)
             copy.start()
             pending.append(copy)
 
-    def relay_act(slot, half):
-        pass_on(slot, 2, over, mate, half).wait_recv()
-        copy = pass_on(slot, 2, over, mate, half)
-        copy.start()
-        pending.append(copy)
-
-    def contract_act(slot, weight, half):
-        pass_on(slot, 1, mate, mate, half).wait_recv()
-        pass_on(slot, 2, diag, mate, half).wait_recv()
+    def contract_act(slot, weight, half=None):
+        listing, begin, length = span_of(half)
+        for n in listing:
+            pass_on(slot, 1, mate, mate, n).wait_recv()
+            pass_on(slot, 2, diag, mate, n).wait_recv()
         total = None
         for chunk in range(4):
             part = jnp.dot(
-                act[slot, chunk, pl.ds(half * window, window), :],
+                act[slot, chunk, pl.ds(begin, length), :],
                 weight[chunk * hidden : (chunk + 1) * hidden, :],
                 preferred_element_type=f32,
             )
@@ -533,20 +547,18 @@
             eout.at[k, here], eback.at[b, here], e_s.at[k, half], e_r.at[b, half], order[k], t
         )
 
-    def finish(k, half):
-        here = pl.ds(half * window, window)
-        eout[k, here, :] = contract_act(k, dn_v, half).astype(bf16)
-        copy = give_back(k, s, half)
-        copy.start()
-        pending.append(copy)
-
-    def expert(k, half):
+    def finish(k, half=None):
+        listing, begin, length = span_of(half)
+        eout[k, pl.ds(begin, length), :] = contract_act(k, dn_v, half).astype(bf16)
+        for n in listing:
+            copy = give_back(k, s, n)
+            copy.start()
+            pending.append(copy)
+
+    def expert(k, half=None):
         normalize(k, half)
         activate(k, gu_v, half)
-
-    def each(step, *given):
-        for n in halves:
-            step(*given, n)
+        ship(k, half)
 
     early, late = halves[0], halves[-1]
     arrive(1)
@@ -556,38 +568,38 @@
     relay(1)
     loads[2].wait()
     loads[3].wait()
-    each(expert, 1)
+    expert(1)
     arrive(3, early)
     arrive_over(2)
-    each(expert, 0)
+    normalize(0)
+    activate(0, gu_v)
+    relay(2)
     loads[4].wait()
     loads[5].wait()
-    each(activate, 4, sgu_v)
-    relay(2)
-    each(expert, 2)
-    each(relay_act, 1)
+    activate(4, sgu_v)
+    expert(2)
+    relay_act(1)
     loads[6].wait()
-    each(finish, 1)
+    finish(1)
     arrive(3, late)
     arrive_over(3)
-    each(relay_act, 0)
-    each(relay_act, 4)
     relay(3, early)
     expert(3, early)
-    each(relay_act, 2)
-    each(finish, 2)
+    relay_act(2)
+    finish(2)
     relay(3, late)
     expert(3, late)
-    for n in halves:
-        eout[0, pl.ds(n * window, window), :] = contract_act(0, dn_v, n).astype(bf16)
+    ship(0)
+    ship(4)
     relay_act(3, early)
     finish(3, early)
-    loads[7].wait()
-    for n in halves:
-        here = pl.ds(n * window, window)
-        acc[here, :] = contract_act(4, sdn_v, n)
     relay_act(3, late)
     finish(3, late)
+    relay_act(0)
+    relay_act(4)
+    eout[0] = contract_act(0, dn_v).astype(bf16)
+    loads[7].wait()
+    acc[...] = contract_act(4, sdn_v)
 
     def weight_of(e):
         total = jnp.zeros((rows, 1), f32)

time: 74 us -> 70.2 us (0.949)
  Pallas kernels: 72.2 us -> 68.4 us
    pallas_call x1, Pallas kernels: 72.2 us -> 68.4 us  [layer(): pl.pallas_call(functools.partial(fused_kernel, (rows, cols, width, WINDOW...]
where the time goes in v5:
time: 70.2 us; the launch traced here: 70.1 us
  Pallas kernels  68.4 us (97%)
  local copies, waits for them, and re-layouts  1.67 us (2%)
    pallas_call x1, Pallas kernels, layer(): pl.pallas_call(functools.partial(fused_kernel, (rows, cols, width, WINDOW...  68.4 us
    unnamed x1, local copies, waits for them, and re-layouts  1.67 us

profile of v5, /device:TPU:0, one launch (start us, length us, event | category | flops | bytes accessed | tf_op | source)
XLA Modules:
  0.0 70.1 jit_solution(5997246090204263297)
XLA Ops:
  0.0 68.4 %shard_map.154 = bf16[256,512]{1,0:T(8,128)(2,1)} custom-call(bf16[256,2048]{1,0:T(8,128)(2,1)} %res_hbm.1, bf16[256,256]{1,0:T(8,128)(2,1)} %q_ref.1, bf16[256,128]{1,0:T(8,128)(2,1)} %k_ref.1, bf16[256,128]{1,0:T(8,128)(2,1)} %v_ref.1, s32[1,256]{1,0:T(1,128)} %bitcast.7, s32[2,256]{1,0:T(2,128)} %bitcast.5, f32[2,256]{1,0:T(2,128)} %bitcast.6, ...), custom_call_target="tpu_custom_call" | custom-call | tf_op jit(solution)/shard_map/pallas_call | solution.py:695
  68.4 1.7 %copy.18 = bf16[256,512]{1,0:T(8,128)(2,1)} copy(bf16[256,512]{1,0:T(8,128)(2,1)} %shard_map.154) | data formatting | bytes 524288

commit v6 on v5

--- a/solution.py
+++ b/solution.py
@@ -227,6 +227,14 @@
             device_id_type=MESH,
         )
 
+    barrier = pltpu.get_barrier_semaphore()
+    pl.semaphore_signal(barrier, inc=1, device_id={"sp": s, "tp": mate}, device_id_type=MESH)
+    pl.semaphore_signal(barrier, inc=1, device_id={"sp": s, "tp": over}, device_id_type=MESH)
+    for step in range(1, 4):
+        pl.semaphore_signal(
+            barrier, inc=1, device_id={"sp": (s + step) % 4, "tp": t}, device_id_type=MESH
+        )
+
     own_cols = pl.ds(pl.multiple_of(t * cols, cols), cols)
     loads = [
         pltpu.make_async_copy(wo_hbm, wo_v, w_sem.at[0]),
@@ -247,15 +255,6 @@
     aux_rows[1 : 1 + top_count, :] = routes_ref[...].astype(f32)
     aux_rows[1 + top_count : 1 + 2 * top_count, :] = rw_ref[...]
     marks_v[...] = jnp.broadcast_to(aux_rows[0:1, pl.ds(rows - window, window)], (8, window))
-    barrier = pltpu.get_barrier_semaphore()
-    pl.semaphore_signal(barrier, inc=1, device_id={"sp": s, "tp": mate}, device_id_type=MESH)
-    pl.semaphore_signal(barrier, inc=1, device_id={"sp": s, "tp": over}, device_id_type=MESH)
-    for step in range(1, 4):
-        pl.semaphore_signal(
-            barrier, inc=1, device_id={"sp": (s + step) % 4, "tp": t}, device_id_type=MESH
-        )
-    pl.semaphore_wait(barrier, 5)
-
     def marks_across(n):
         return aux_rows[0:1, pl.ds(n * window, window)]
 
@@ -266,11 +265,6 @@
         remote(v_ref.at[tail], vh, halo_s.at[1], halo_r.at[1], up_sp, t),
         remote(marks_v, mh, halo_s.at[2], halo_r.at[2], up_sp, t),
     ]
-
-    @pl.when(s < 3)
-    def _():
-        for copy in halos:
-            copy.start()
 
     @pl.when(s == 0)
     def _():
@@ -330,6 +324,14 @@
         )
 
     halves = list(range(rows // window))[::-1]
+    attend(halves[0])
+    pl.semaphore_wait(barrier, 5)
+
+    @pl.when(s < 3)
+    def _():
+        for copy in halos:
+            copy.start()
+
     pending = []
     first = {}
     second = {}
@@ -341,8 +343,9 @@
                 for copy in halos:
                     copy.wait_recv()
 
-        attend(n)
-        if n == halves[0]:
+        if n != halves[0]:
+            attend(n)
+        else:
             loads[0].wait()
             for load in loads[2:]:
                 load.start()
@@ -681,7 +684,7 @@
     n_sp, n_tp = lax.axis_size("sp"), lax.axis_size("tp")
     capacity = 2 * rows * routes.shape[1] // n_sp
     hidden = expert_gate.shape[2]
-    if n_sp != 4 or n_tp != 4 or capacity < rows or shared_gate.shape[1] != hidden:
+    if n_sp != 4 or n_tp != 4 or capacity < rows or rows < 2 * WINDOW or shared_gate.shape[1] != hidden:
         return shards(*arguments)
     cols = width // n_tp
     heads = queries.shape[1] // HEAD_DIM

time: 70.2 us -> 70.1 us (level)
  no operation moved by 1% of the time
where the time goes in v6:
time: 70.1 us; the launch traced here: 70 us
  Pallas kernels  68.3 us (97%)
  local copies, waits for them, and re-layouts  1.67 us (2%)
    pallas_call x1, Pallas kernels, layer(): pl.pallas_call(functools.partial(fused_kernel, (rows, cols, width, WINDOW...  68.3 us
    unnamed x1, local copies, waits for them, and re-layouts  1.67 us

profile of v6, /device:TPU:0, one launch (start us, length us, event | category | flops | bytes accessed | tf_op | source)
XLA Modules:
  0.0 70.0 jit_solution(4378839192913054670)
XLA Ops:
  0.0 68.3 %shard_map.154 = bf16[256,512]{1,0:T(8,128)(2,1)} custom-call(bf16[256,2048]{1,0:T(8,128)(2,1)} %res_hbm.1, bf16[256,256]{1,0:T(8,128)(2,1)} %q_ref.1, bf16[256,128]{1,0:T(8,128)(2,1)} %k_ref.1, bf16[256,128]{1,0:T(8,128)(2,1)} %v_ref.1, s32[1,256]{1,0:T(1,128)} %bitcast.7, s32[2,256]{1,0:T(2,128)} %bitcast.5, f32[2,256]{1,0:T(2,128)} %bitcast.6, ...), custom_call_target="tpu_custom_call" | custom-call | tf_op jit(solution)/shard_map/pallas_call | solution.py:698
  68.3 1.7 %copy.18 = bf16[256,512]{1,0:T(8,128)(2,1)} copy(bf16[256,512]{1,0:T(8,128)(2,1)} %shard_map.154) | data formatting | bytes 524288
